TPU v7x, 32 devices: a whole 2x2x4 slice. The times are simulated.
32 devices in a mesh: fs: 8 (over z, y), tp: 4 (over x, core).
Axes of the slice: x: 2, y: 2, z: 4, core: 2. Of those that a mesh axis runs over, the one named last changes fastest.
Arguments:
- inputs: bfloat16 [48, 4096], P('fs', 'tp'), may hold values from -0.875 to 0.875
- cotangent: bfloat16 [48, 4096], P('fs', 'tp'), may hold values from -8 to 8
- pre_act: bfloat16 [48, 16384], P(None, 'fs'), may hold values from -3 to 3
- w_up: bfloat16 [4096, 16384], P('tp', 'fs'), may hold values from -0.046875 to 0.046875
- w_down: bfloat16 [16384, 4096], P('fs', 'tp'), may hold values from -0.09375 to 0.09375
Outputs:
- grad_input: bfloat16 [48, 4096], P('fs', 'tp')
- grad_up: float32 [4096, 16384], P('tp', 'fs')
- grad_down: float32 [16384, 4096], P('fs', 'tp')
All inputs are finite; a program needn't handle non-finite values.
Results may differ from a plain program's by a relative error of at most 0.017.
Values may be sent and summed in bfloat16 or wider, within the bound.
A program may use at most 64 MiB of HBM per device.

v0:
```python
import jax
import jax.numpy as jnp
from jax import lax
from jax.sharding import PartitionSpec as P


def body(inputs, cotangent, pre_act, w_up, w_down):
    active = jax.nn.relu(pre_act.astype(jnp.float32))
    squared = jnp.square(active).astype(jnp.bfloat16)
    piece = lax.all_gather(cotangent, "fs", axis=0, tiled=True)
    term = lax.dot_general(
        piece, w_down, (((1,), (1,)), ((), ())), preferred_element_type=jnp.float32
    )
    hidden_part = term
    grad_acc = lax.dot_general(
        squared, piece, (((0,), (0,)), ((), ())), preferred_element_type=jnp.float32
    )
    hidden_part, grad_down = (hidden_part, grad_acc)
    hidden = lax.psum(hidden_part.astype(jnp.bfloat16), "tp").astype(jnp.float32)
    grad_pre = (2.0 * active * hidden).astype(jnp.bfloat16)
    grad_rows = grad_pre
    grad_up = lax.dot_general(
        lax.all_gather(inputs, "fs", axis=0, tiled=True),
        grad_rows,
        (((0,), (0,)), ((), ())),
        preferred_element_type=jnp.float32,
    )
    grad_rows = grad_pre
    grad_input = lax.psum_scatter(
        lax.dot_general(
            grad_rows, w_up, (((1,), (1,)), ((), ())), preferred_element_type=jnp.float32
        ),
        "fs",
        scatter_dimension=0,
        tiled=True,
    ).astype(jnp.bfloat16)
    return (grad_input, grad_up, grad_down)


def solution(mesh):
    return jax.shard_map(
        body,
        mesh=mesh,
        in_specs=(P("fs", "tp"), P("fs", "tp"), P(None, "fs"), P("tp", "fs"), P("fs", "tp")),
        out_specs=(P("fs", "tp"), P("tp", "fs"), P("fs", "tp")),
        check_vma=False,
    )
```

profile of v0, /device:TPU:0, one launch (start us, length us, event | category | flops | bytes accessed | tf_op | source)
XLA Modules:
  0.0 132.2 jit_solution(8270654237708028244)
XLA Ops:
  7.2 0.0 copy-start
  7.2 0.0 all-reduce.4.cloned.1.call-start
  7.2 32.7 %all-gather = bf16[8,6,1024]{2,1,0:T(8,128)(2,1)S(1)} all-gather(bf16[1,6,1024]{2,1,0:T(8,128)(2,1)} %bitcast.12), channel_id=1, replica_groups=mesh['fs'=8,'tp'=4] {'fs'}, dimensions={0}, use_global_device_ids=true | all-gather | bytes 110592 | tf_op jit(solution)/shard_map/all_gather | solution.py:10
  39.9 4.2 %convolution_convert_fusion = bf16[48,2048]{1,0:T(8,128)(2,1)} fusion(bf16[48,1024]{1,0:T(8,128)(2,1)S(1)} %reshape.7, bf16[2048,1024]{1,0:T(8,128)(2,1)} %param.9), kind=kOutput, calls=%fused_computation.1 | convolution fusion | flops 201424896 | bytes 4489216 | tf_op jit(solution)/shard_map/dot_general | solution.py:11
  44.2 0.0 all-reduce.4.cloned.1.call-update
  44.2 0.0 copy-done
  44.2 0.0 copy-start.2
  44.2 0.0 copy-start.3
  44.2 4.7 %fusion.1 = f32[2048,1024]{1,0:T(8,128)} fusion(bf16[48,1024]{1,0:T(8,128)(2,1)S(1)} %reshape.7, bf16[48,2048]{1,0:T(8,128)(2,1)S(1)} %copy-done), kind=kOutput, calls=%fused_computation.5 | convolution fusion | flops 201719808 | bytes 8683520 | tf_op jit(solution)/shard_map/dot_general | solution.py:15
  48.9 0.0 copy-done.2
  48.9 30.5 %all-gather.1 = bf16[8,6,1024]{2,1,0:T(8,128)(2,1)S(1)} all-gather(bf16[1,6,1024]{2,1,0:T(8,128)(2,1)S(1)} %bitcast.13), channel_id=1, replica_groups=mesh['fs'=8,'tp'=4] {'fs'}, dimensions={0}, use_global_device_ids=true | all-gather | bytes 110592 | tf_op jit(solution)/shard_map/all_gather | solution.py:23
  79.5 0.0 copy-done.3
  79.5 0.6 dynamic-slice.4
  80.7 0.0 all-reduce.4.cloned.1.call-done
  80.8 0.0 copy-start.1
  80.8 3.7 %fusion.3 = f32[48,1024]{1,0:T(8,128)S(1)} fusion(bf16[1024,2048]{1,0:T(8,128)(2,1)} %param.8, bf16[48,2048]{1,0:T(8,128)(2,1)} %all-reduce.4.cloned.1.call-done, bf16[48,2048]{1,0:T(8,128)(2,1)S(1)} %copy-done), kind=kOutput, calls=%fused_computation.8 | convolution fusion | flops 201916416 | bytes 4784128 | tf_op jit(solution)/shard_map/dot_general | solution.py:30
  84.5 23.7 %fusion = f32[8,1024]{1,0:T(8,128)S(1)} fusion(f32[48,1024]{1,0:T(8,128)S(1)} %fusion.3), kind=kCustom, calls=%all-reduce-scatter | all-reduce-scatter fusion | flops 65537 | bytes 229888
  108.2 1.3 collective-permute-start
  109.5 1.3 collective-permute-start.1
  110.8 0.0 copy-done.1
  110.8 4.5 %convolution_bitcast_fusion = f32[1024,2048]{0,1:T(8,128)} fusion(bf16[48,1024]{1,0:T(8,128)(2,1)S(1)} %reshape.9, bf16[48,2048]{1,0:T(8,128)(2,1)S(1)} %copy-done.1, bf16[48,2048]{1,0:T(8,128)(2,1)S(1)} %copy-done), kind=kOutput, calls=%fused_computation | convolution fusion | flops 201916416 | bytes 8880128 | tf_op jit(solution)/shard_map/dot_general | solution.py:22
  115.3 9.1 %copy.10 = f32[1024,2048]{1,0:T(8,128)} copy(f32[1024,2048]{0,1:T(8,128)} %convolution_bitcast_fusion) | data formatting | bytes 16777216
  124.4 0.0 collective-permute-done.1
  124.4 0.0 collective-permute-done
  124.4 0.2 concatenate
  124.7 0.6 dynamic-slice_convert_fusion
  (4 shorter events, 0.1 us)
Async XLA Ops:
  7.2 37.0 %copy-start = (bf16[48,2048]{1,0:T(8,128)(2,1)S(1)}, bf16[48,2048]{1,0:T(8,128)(2,1)}, u32[]{:S(2)}) copy-start(bf16[48,2048]{1,0:T(8,128)(2,1)} %param.7) | copy-start | bytes 589828
  7.2 73.6 %all-reduce.4.cloned.1.call-start = ((), (), s32[]{:S(2)}) async-start(), calls=%async_computation | async-start | bytes 393216 | tf_op jit(solution)/shard_map/psum | solution.py:19
  44.2 4.7 %copy-start.2 = (bf16[6,1024]{1,0:T(8,128)(2,1)S(1)}, bf16[6,1024]{1,0:T(8,128)(2,1)}, u32[]{:S(2)}) copy-start(bf16[6,1024]{1,0:T(8,128)(2,1)} %param.5) | copy-start | bytes 36868
  44.2 35.2 %copy-start.3 = (u32[32]{0:T(128)S(1)}, u32[32]{0:T(128)}, u32[]{:S(2)}) copy-start(u32[32]{0:T(128)} %constant.9) | copy-start | bytes 388
  80.8 30.1 %copy-start.1 = (bf16[48,2048]{1,0:T(8,128)(2,1)S(1)}, bf16[48,2048]{1,0:T(8,128)(2,1)}, u32[]{:S(2)}) copy-start(bf16[48,2048]{1,0:T(8,128)(2,1)} %all-reduce.4.cloned.1.call-done) | copy-start | bytes 589828
  108.2 16.2 %collective-permute-start = (bf16[8,1024]{1,0:T(8,128)(2,1)S(1)}, bf16[8,1024]{1,0:T(8,128)(2,1)S(1)}, u32[]{:S(2)}, u32[]{:S(2)}) collective-permute-start(bf16[8,1024]{1,0:T(8,128)(2,1)S(1)} %convert), channel_id=1, source_target_pairs={{0,4},{4,8},{8,12},{12,16},{16,20},{20,24},{24,28},{1,5},{5,9},{9,... | collective-permute-start | bytes 49160
  109.5 14.9 %collective-permute-start.1 = (bf16[6,1024]{1,0:T(8,128)(2,1)S(1)}, bf16[6,1024]{1,0:T(8,128)(2,1)S(1)}, u32[]{:S(2)}, u32[]{:S(2)}) collective-permute-start(bf16[6,1024]{1,0:T(8,128)(2,1)S(1)} %slice), channel_id=1, source_target_pairs={{0,8},{4,12},{8,16},{12,20},{16,24},{20,28},{1,9},{5,13},{9,17},{1... | collective-permute-start | bytes 36872
Sparse Core Ops, SparseCore 0:
  44.3 32.9 all-reduce.3
where the time goes:
time: 133 us; the launch traced here: 132 us
  blocking collectives  86.9 us (65%)
  matrix products  17.1 us (13%)
  between operations  14.8 us (11%)
  local copies, waits for them, and re-layouts  10.7 us (8%)
  starting transfers between devices  2.62 us (2%)
    all_gather x1, blocking collectives, body(): piece = lax.all_gather(cotangent, 'fs', axis=0, tiled=True)  32.7 us
    all_gather x1, blocking collectives, body(): lax.all_gather(inputs, 'fs', axis=0, tiled=True)  30.5 us
    unnamed x1, blocking collectives  23.7 us
    unnamed x14, local copies, waits for them, and re-layouts  10.1 us
    dot_general x1, matrix products, body(): lax.dot_general(squared, piece, (((0,), (0,)), ((), ())), preferred_eleme...  4.68 us
    dot_general x1, matrix products, body(): lax.dot_general(lax.all_gather(inputs, 'fs', axis=0, tiled=True), grad_ro...  4.5 us
    dot_general x1, matrix products, body(): lax.dot_general(piece, w_down, (((1,), (1,)), ((), ())), preferred_elemen...  4.24 us
    dot_general x1, matrix products, body(): lax.dot_general(grad_rows, w_up, (((1,), (1,)), ((), ())), preferred_elem...  3.7 us
  transfers between devices with their start and end apart: 3, of which 0 were waited for; matrix products, arithmetic and copies ran while one was open for 14% of the time, Pallas kernels for 0%

commit v1 on v0

v1 whole, which is shorter than its diff:
```python
import functools

import jax
import jax.numpy as jnp
from jax import lax
from jax.experimental import pallas as pl
from jax.experimental.pallas import tpu as pltpu
from jax.sharding import PartitionSpec as P

F32, BF16 = jnp.float32, jnp.bfloat16
SLAB = 8
NT = (((1,), (1,)), ((), ()))
TN = (((0,), (0,)), ((), ()))
NN = (((1,), (0,)), ((), ()))


def dot(a, b, dims):
    return lax.dot_general(a, b, dims, preferred_element_type=F32)


def exchange(
    n,
    chips,
    chunks,
    cot_ref,
    in_ref,
    pre_ref,
    wu_ref,
    wd_ref,
    cot_out,
    in_out,
    gp_out,
    gi_out,
    cot_v,
    in_v,
    pre_v,
    wu_v,
    wd_v,
    cot_g,
    in_g,
    spread,
    own,
    p1_s,
    p1_r,
    p2_s,
    p2_r,
    rs_s,
    rs_r,
    local,
    cs,
    cr,
    is_,
    ir,
    s1,
    r1,
    s2,
    r2,
    s3,
    r3,
    s4,
    r4,
):
    me = lax.axis_index("fs")
    tp = lax.axis_index("tp")
    core = lax.rem(tp, 2)
    rows = cot_v.shape[0]
    tokens = n * rows
    width = wd_v.shape[1]
    fs_peer = [None] + [lax.rem(me + k, n) for k in range(1, n)]
    partner = tp + 1 - 2 * core
    x_peer = [None] + [lax.rem(tp + 2 * k, 2 * chips) for k in range(1, chips)]
    targets = (
        [{"fs": p} for p in fs_peer[1:]]
        + [{"tp": partner}]
        + [{"tp": p} for p in x_peer[1:]]
    )

    barrier = pltpu.get_barrier_semaphore()
    for t in targets:
        pl.semaphore_signal(barrier, inc=1, device_id=t)

    load_cot = pltpu.make_async_copy(cot_ref, cot_v, local.at[0])
    load_in = pltpu.make_async_copy(in_ref, in_v, local.at[1])
    load_cot.start()
    load_in.start()
    load_wd, load_pre, load_wu = [], [], []
    for j in range(2 * chunks):
        load_wd.append(
            pltpu.make_async_copy(
                wd_ref.at[pl.ds(j * width, width)], wd_v.at[j], local.at[4 + j]
            )
        )
        load_wd[-1].start()
    for j in range(2 * chunks):
        load_pre.append(
            pltpu.make_async_copy(
                pre_ref.at[:, pl.ds(j * width, width)],
                pre_v.at[j],
                local.at[4 + 2 * chunks + j],
            )
        )
        load_pre[-1].start()
    for j in range(2 * chunks):
        load_wu.append(
            pltpu.make_async_copy(
                wu_ref.at[:, pl.ds(j * width, width)],
                wu_v.at[j],
                local.at[4 + 4 * chunks + j],
            )
        )
        load_wu[-1].start()
    spread[...] = jnp.zeros_like(spread)
    load_cot.wait()
    load_in.wait()
    own_cot = pltpu.make_async_copy(cot_v, cot_g.at[me], local.at[2])
    own_in = pltpu.make_async_copy(in_v, in_g.at[me], local.at[3])
    own_cot.start()
    own_in.start()

    pl.semaphore_wait(barrier, len(targets))
    sends_c, sends_i = [], []
    for k in range(1, n):
        copy = pltpu.make_async_remote_copy(
            cot_v, cot_g.at[me], cs.at[k], cr.at[k], device_id={"fs": fs_peer[k]}
        )
        copy.start()
        sends_c.append(copy)
    for k in range(1, n):
        copy = pltpu.make_async_remote_copy(
            in_v, in_g.at[me], is_.at[k], ir.at[k], device_id={"fs": fs_peer[k]}
        )
        copy.start()
        sends_i.append(copy)

    def picker(shape, token_dim):
        t = lax.broadcasted_iota(jnp.int32, shape, token_dim)
        j = lax.broadcasted_iota(jnp.int32, shape, 1 - token_dim)
        q, r = j // SLAB, j % SLAB
        return ((t == q * rows + r) & (r < rows)).astype(F32).astype(BF16)

    pick = picker((tokens, n * SLAB), 0)
    place = picker((n * SLAB, tokens), 1)

    def gathered(ref):
        for s in range(n):
            spread[s * SLAB : s * SLAB + rows, :] = ref[s].astype(F32)
        return dot(pick, spread[...].astype(BF16), NN).astype(BF16)

    own_cot.wait()
    for copy in load_wd:
        copy.wait()
    for copy in sends_c:
        copy.wait_recv()
    cot_out[...] = gathered(cot_g)

    first, other = core * chunks, (1 - core) * chunks
    send1 = []
    for j in range(chunks):
        p1_s[j] = dot(cot_out[...], wd_v[other + j], NT).astype(BF16)
        copy = pltpu.make_async_remote_copy(
            p1_s.at[j], p1_r.at[j], s1.at[j], r1.at[j], device_id={"tp": partner}
        )
        copy.start()
        send1.append(copy)
    for j in range(chunks):
        own[j] = dot(cot_out[...], wd_v[first + j], NT)
    send2 = []
    for j in range(chunks):
        send1[j].wait_recv()
        total = own[j] + p1_r[j].astype(F32)
        own[j] = total
        p2_s[j] = total.astype(BF16)
        for k in range(1, chips):
            copy = pltpu.make_async_remote_copy(
                p2_s.at[j],
                p2_r.at[k - 1, j],
                s2.at[k - 1, j],
                r2.at[k - 1, j],
                device_id={"tp": x_peer[k]},
            )
            copy.start()
            send2.append(copy)

    own_in.wait()
    for copy in sends_i:
        copy.wait_recv()
    in_out[...] = gathered(in_g)
    for copy in load_pre:
        copy.wait()
    for copy in load_wu:
        copy.wait()

    send3 = []
    for j in range(chunks):
        hidden = own[j]
        for k in range(1, chips):
            send2[j * (chips - 1) + k - 1].wait_recv()
            hidden = hidden + p2_r[k - 1, j].astype(F32)
        active = jnp.maximum(pre_v[first + j].astype(F32), 0.0)
        gp_out[first + j] = (2.0 * active * hidden).astype(BF16)
        copy = pltpu.make_async_remote_copy(
            gp_out.at[first + j],
            gp_out.at[first + j],
            s3.at[j],
            r3.at[j],
            device_id={"tp": partner},
        )
        copy.start()
        send3.append(copy)
    acc = None
    for j in range(chunks):
        term = dot(gp_out[first + j], wu_v[first + j], NT)
        acc = term if acc is None else acc + term
    for j in range(chunks):
        pltpu.make_async_remote_copy(
            gp_out.at[other + j],
            gp_out.at[other + j],
            s3.at[j],
            r3.at[j],
            device_id={"tp": partner},
        ).wait_recv()
        acc = acc + dot(gp_out[other + j], wu_v[other + j], NT)
    slabs = dot(place, acc.astype(BF16), NN)
    for s in range(n):
        rs_s[s] = slabs[s * SLAB : s * SLAB + rows, :].astype(BF16)
    send4 = []
    for k in range(1, n):
        copy = pltpu.make_async_remote_copy(
            rs_s.at[fs_peer[k]],
            rs_r.at[k - 1],
            s4.at[k],
            r4.at[k],
            device_id={"fs": fs_peer[k]},
        )
        copy.start()
        send4.append(copy)
    for copy in sends_c + sends_i + send1 + send2 + send3:
        copy.wait_send()
    total = rs_s[me].astype(F32)
    for k in range(1, n):
        send4[k - 1].wait_recv()
        total = total + rs_r[k - 1].astype(F32)
    gi_out[...] = total.astype(BF16)
    for copy in send4:
        copy.wait_send()


def outer(chunks, cot_ref, in_ref, pre_ref, gp_ref, gi_ref, gi_out, gu_out, gd_out):
    @pl.when(pl.program_id(0) == 0)
    def _():
        gi_out[...] = gi_ref[...]

    active = jnp.maximum(pre_ref[...].astype(F32), 0.0)
    act = (active * active).astype(BF16)
    gd_out[...] = dot(act, cot_ref[...], TN)
    width = gp_ref.shape[2]
    for j in range(2 * chunks):
        gu_out[:, j * width : (j + 1) * width] = dot(in_ref[...], gp_ref[j], TN)


def fused(n, ntp, inputs, cotangent, pre_act, w_up, w_down):
    rows, d = inputs.shape
    tokens, ff = pre_act.shape
    chips = ntp // 2
    chunks = 2 if (ff // 2) % 256 == 0 else 1
    width = ff // 2 // chunks
    hbm = pl.BlockSpec(memory_space=pl.ANY)
    vmem = pl.BlockSpec(memory_space=pltpu.VMEM)
    dma = pltpu.SemaphoreType.DMA
    cot, full, gp, gi = pl.pallas_call(
        functools.partial(exchange, n, chips, chunks),
        out_shape=(
            jax.ShapeDtypeStruct((tokens, d), BF16),
            jax.ShapeDtypeStruct((tokens, d), BF16),
            jax.ShapeDtypeStruct((2 * chunks, tokens, width), BF16),
            jax.ShapeDtypeStruct((rows, d), BF16),
        ),
        in_specs=[hbm] * 5,
        out_specs=(vmem,) * 4,
        scratch_shapes=[
            pltpu.VMEM((rows, d), BF16),
            pltpu.VMEM((rows, d), BF16),
            pltpu.VMEM((2 * chunks, tokens, width), BF16),
            pltpu.VMEM((2 * chunks, d, width), BF16),
            pltpu.VMEM((2 * chunks, width, d), BF16),
            pltpu.VMEM((n, rows, d), BF16),
            pltpu.VMEM((n, rows, d), BF16),
            pltpu.VMEM((n * SLAB, d), F32),
            pltpu.VMEM((chunks, tokens, width), F32),
            pltpu.VMEM((chunks, tokens, width), BF16),
            pltpu.VMEM((chunks, tokens, width), BF16),
            pltpu.VMEM((chunks, tokens, width), BF16),
            pltpu.VMEM((chips - 1, chunks, tokens, width), BF16),
            pltpu.VMEM((n, rows, d), BF16),
            pltpu.VMEM((n - 1, rows, d), BF16),
            dma((4 + 6 * chunks,)),
            dma((n,)),
            dma((n,)),
            dma((n,)),
            dma((n,)),
            dma((chunks,)),
            dma((chunks,)),
            dma((chips - 1, chunks)),
            dma((chips - 1, chunks)),
            dma((chunks,)),
            dma((chunks,)),
            dma((n,)),
            dma((n,)),
        ],
        compiler_params=pltpu.CompilerParams(collective_id=0, has_side_effects=True),
    )(cotangent, inputs, pre_act, w_up, w_down)
    steps = 8
    fixed = lambda i: (0, 0)
    return pl.pallas_call(
        functools.partial(outer, chunks),
        grid=(steps,),
        out_shape=(
            jax.ShapeDtypeStruct((rows, d), BF16),
            jax.ShapeDtypeStruct((d, ff), F32),
            jax.ShapeDtypeStruct((ff, d), F32),
        ),
        in_specs=[
            pl.BlockSpec((tokens, d), fixed),
            pl.BlockSpec((tokens, d // steps), lambda i: (0, i)),
            pl.BlockSpec((tokens, ff // steps), lambda i: (0, i)),
            pl.BlockSpec((2 * chunks, tokens, width), lambda i: (0, 0, 0)),
            pl.BlockSpec((rows, d), fixed),
        ],
        out_specs=(
            pl.BlockSpec((rows, d), fixed),
            pl.BlockSpec((d // steps, ff), lambda i: (i, 0)),
            pl.BlockSpec((ff // steps, d), lambda i: (i, 0)),
        ),
    )(cot, full, pre_act, gp, gi)


def plain(inputs, cotangent, pre_act, w_up, w_down):
    active = jax.nn.relu(pre_act.astype(F32))
    squared = jnp.square(active).astype(BF16)
    piece = lax.all_gather(cotangent, "fs", axis=0, tiled=True)
    grad_down = dot(squared, piece, TN)
    hidden = lax.psum(dot(piece, w_down, NT).astype(BF16), "tp").astype(F32)
    grad_pre = (2.0 * active * hidden).astype(BF16)
    grad_up = dot(lax.all_gather(inputs, "fs", axis=0, tiled=True), grad_pre, TN)
    grad_input = lax.psum_scatter(
        dot(grad_pre, w_up, NT), "fs", scatter_dimension=0, tiled=True
    ).astype(BF16)
    return (grad_input, grad_up, grad_down)


def solution(mesh):
    n, ntp = mesh.shape["fs"], mesh.shape["tp"]

    def body(inputs, cotangent, pre_act, w_up, w_down):
        rows, d = inputs.shape
        tokens, ff = pre_act.shape
        if (
            1 < n <= 16
            and ntp > 2
            and ntp % 2 == 0
            and rows <= SLAB
            and tokens % 16 == 0
            and d % 1024 == 0
            and ff % 1024 == 0
        ):
            return fused(n, ntp, inputs, cotangent, pre_act, w_up, w_down)
        return plain(inputs, cotangent, pre_act, w_up, w_down)

    return jax.shard_map(
        body,
        mesh=mesh,
        in_specs=(P("fs", "tp"), P("fs", "tp"), P(None, "fs"), P("tp", "fs"), P("fs", "tp")),
        out_specs=(P("fs", "tp"), P("tp", "fs"), P("fs", "tp")),
        check_vma=False,
    )
```

time: 133 us -> 35.1 us (0.26)
  blocking collectives: 86.9 us -> 0 us
  Pallas kernels: 0 us -> 34 us
  matrix products: 17.1 us -> 0 us
  between operations: 14.8 us -> 0.64 us
  local copies, waits for them, and re-layouts: 10.7 us -> 0 us
  starting transfers between devices: 2.62 us -> 0 us
    all_gather x2 -> x0, blocking collectives: 63.2 us -> none  [the longest x1 32.7 us: body(): piece = lax.all_gather(cotangent, 'fs', axis=0, tiled=True)]
    pallas_call x0 -> x2, Pallas kernels: none -> 34 us  [the longest x1 25.6 us: fused(): pl.pallas_call(functools.partial(exchange, n, chips, chunks), out_shape=(...]
    unnamed x1 -> x0, blocking collectives: 23.7 us -> none
    dot_general x4 -> x0, matrix products: 17.1 us -> none  [the longest x1 4.68 us: body(): lax.dot_general(squared, piece, (((0,), (0,)), ((), ())), preferred_eleme...]
    unnamed x14 -> x0, local copies, waits for them, and re-layouts: 10.1 us -> none
    unnamed x2 -> x0, starting transfers between devices: 2.58 us -> none
  transfers between devices with their start and end apart: 3 -> 0, of which waited for: 0 -> 0; matrix products, arithmetic and copies ran while one was open for 14% -> 0% of each run, Pallas kernels for 0% -> 0%
where the time goes in v1:
time: 35.1 us; the launch traced here: 34.6 us
  Pallas kernels  34 us (97%)
  between operations  0.64 us (2%)
    pallas_call x1, Pallas kernels, fused(): pl.pallas_call(functools.partial(exchange, n, chips, chunks), out_shape=(...  25.6 us
    pallas_call x1, Pallas kernels, fused(): pl.pallas_call(functools.partial(outer, chunks), grid=(steps,), out_shape...  8.37 us

profile of v1, /device:TPU:0, one launch (start us, length us, event | category | flops | bytes accessed | tf_op | source)
XLA Modules:
  0.0 34.6 jit_solution(11525870768713829644)
XLA Ops:
  0.6 25.6 %shard_map.76 = (bf16[48,1024]{1,0:T(8,128)(2,1)}, bf16[48,1024]{1,0:T(8,128)(2,1)}, bf16[4,48,512]{2,1,0:T(8,128)(2,1)}, bf16[6,1024]{1,0:T(8,128)(2,1)}) custom-call(bf16[6,1024]{1,0:T(8,128)(2,1)} %cot_ref.1, bf16[6,1024]{1,0:T(8,128)(2,1)} %in_ref.1, bf16[48,2048]{1,0:T(8,128)(2,1)} %pre_ref.3, bf16[1024,2048]{1,0:T(8,128)(2,1)} %wu_ref.1, ...), custom_call_target="tpu_custom_call" | custom-call | tf_op jit(solution)/shard_map/pallas_call | solution.py:270
  26.3 8.4 %shard_map.77 = (bf16[6,1024]{1,0:T(8,128)(2,1)}, f32[1024,2048]{1,0:T(8,128)}, f32[2048,1024]{1,0:T(8,128)}) custom-call(bf16[48,1024]{1,0:T(8,128)(2,1)} %get-tuple-element.7.cot_ref, bf16[48,1024]{1,0:T(8,128)(2,1)} %get-tuple-element.8.in_ref, bf16[48,2048]{1,0:T(8,128)(2,1)} %pre_ref.3, bf16[4,48,512]{2,1,0:T(8,128)(2,1)} %get-tuple-element.9.gp_ref, ...), custom_call_target="tpu_custom_call" | custom-call | tf_op jit(solution)/shard_map/pallas_call | solution.py:314

commit v2 on v1

--- a/solution.py
+++ b/solution.py
@@ -29,6 +29,7 @@
     wd_ref,
     cot_out,
     in_out,
+    act_out,
     gp_out,
     gi_out,
     cot_v,
@@ -154,18 +155,17 @@
     cot_out[...] = gathered(cot_g)
 
     first, other = core * chunks, (1 - core) * chunks
-    send1 = []
-    for j in range(chunks):
+    send1, send2 = [], []
+
+    def to_partner(j):
         p1_s[j] = dot(cot_out[...], wd_v[other + j], NT).astype(BF16)
         copy = pltpu.make_async_remote_copy(
             p1_s.at[j], p1_r.at[j], s1.at[j], r1.at[j], device_id={"tp": partner}
         )
         copy.start()
         send1.append(copy)
-    for j in range(chunks):
-        own[j] = dot(cot_out[...], wd_v[first + j], NT)
-    send2 = []
-    for j in range(chunks):
+
+    def to_chips(j):
         send1[j].wait_recv()
         total = own[j] + p1_r[j].astype(F32)
         own[j] = total
@@ -181,12 +181,22 @@
             copy.start()
             send2.append(copy)
 
+    to_partner(0)
+    for j in range(chunks):
+        own[j] = dot(cot_out[...], wd_v[first + j], NT)
+        if j + 1 < chunks:
+            to_partner(j + 1)
+        to_chips(j)
+
     own_in.wait()
     for copy in sends_i:
         copy.wait_recv()
     in_out[...] = gathered(in_g)
     for copy in load_pre:
         copy.wait()
+    for j in range(2 * chunks):
+        active = jnp.maximum(pre_v[j].astype(F32), 0.0)
+        act_out[j] = (active * active).astype(BF16)
     for copy in load_wu:
         copy.wait()
 
@@ -245,17 +255,34 @@
         copy.wait_send()
 
 
-def outer(chunks, cot_ref, in_ref, pre_ref, gp_ref, gi_ref, gi_out, gu_out, gd_out):
-    @pl.when(pl.program_id(0) == 0)
-    def _():
-        gi_out[...] = gi_ref[...]
-
-    active = jnp.maximum(pre_ref[...].astype(F32), 0.0)
-    act = (active * active).astype(BF16)
-    gd_out[...] = dot(act, cot_ref[...], TN)
-    width = gp_ref.shape[2]
-    for j in range(2 * chunks):
-        gu_out[:, j * width : (j + 1) * width] = dot(in_ref[...], gp_ref[j], TN)
+def outer(
+    chunks, cot_v, in_v, act_v, gp_v, gi_v, gi_out, gu_out, gd_out, gu_v, gd_v, sem
+):
+    width = gp_v.shape[2]
+    pieces = []
+
+    def put(src, dst):
+        copy = pltpu.make_async_copy(src, dst, sem.at[len(pieces)])
+        copy.start()
+        pieces.append(copy)
+
+    half = width // 2
+    for j in range(2 * chunks):
+        for h in range(2):
+            rows = pl.ds(j * width + h * half, half)
+            gd_v[rows, :] = dot(act_v[j, :, h * half : (h + 1) * half], cot_v[...], TN)
+            put(gd_v.at[rows], gd_out.at[rows])
+    put(gi_v, gi_out)
+    step = in_v.shape[1] // (4 * chunks)
+    for i in range(4 * chunks):
+        rows = pl.ds(i * step, step)
+        for j in range(2 * chunks):
+            gu_v[rows, j * width : (j + 1) * width] = dot(
+                in_v[:, i * step : (i + 1) * step], gp_v[j], TN
+            )
+        put(gu_v.at[rows], gu_out.at[rows])
+    for copy in pieces:
+        copy.wait()
 
 
 def fused(n, ntp, inputs, cotangent, pre_act, w_up, w_down):
@@ -267,16 +294,17 @@
     hbm = pl.BlockSpec(memory_space=pl.ANY)
     vmem = pl.BlockSpec(memory_space=pltpu.VMEM)
     dma = pltpu.SemaphoreType.DMA
-    cot, full, gp, gi = pl.pallas_call(
+    cot, full, act, gp, gi = pl.pallas_call(
         functools.partial(exchange, n, chips, chunks),
         out_shape=(
-            jax.ShapeDtypeStruct((tokens, d), BF16),
-            jax.ShapeDtypeStruct((tokens, d), BF16),
-            jax.ShapeDtypeStruct((2 * chunks, tokens, width), BF16),
-            jax.ShapeDtypeStruct((rows, d), BF16),
+            pltpu.VMEM((tokens, d), BF16),
+            pltpu.VMEM((tokens, d), BF16),
+            pltpu.VMEM((2 * chunks, tokens, width), BF16),
+            pltpu.VMEM((2 * chunks, tokens, width), BF16),
+            pltpu.VMEM((rows, d), BF16),
         ),
         in_specs=[hbm] * 5,
-        out_specs=(vmem,) * 4,
+        out_specs=(vmem,) * 5,
         scratch_shapes=[
             pltpu.VMEM((rows, d), BF16),
             pltpu.VMEM((rows, d), BF16),
@@ -309,29 +337,21 @@
         ],
         compiler_params=pltpu.CompilerParams(collective_id=0, has_side_effects=True),
     )(cotangent, inputs, pre_act, w_up, w_down)
-    steps = 8
-    fixed = lambda i: (0, 0)
     return pl.pallas_call(
         functools.partial(outer, chunks),
-        grid=(steps,),
         out_shape=(
             jax.ShapeDtypeStruct((rows, d), BF16),
             jax.ShapeDtypeStruct((d, ff), F32),
             jax.ShapeDtypeStruct((ff, d), F32),
         ),
-        in_specs=[
-            pl.BlockSpec((tokens, d), fixed),
-            pl.BlockSpec((tokens, d // steps), lambda i: (0, i)),
-            pl.BlockSpec((tokens, ff // steps), lambda i: (0, i)),
-            pl.BlockSpec((2 * chunks, tokens, width), lambda i: (0, 0, 0)),
-            pl.BlockSpec((rows, d), fixed),
+        in_specs=[vmem] * 5,
+        out_specs=(hbm,) * 3,
+        scratch_shapes=[
+            pltpu.VMEM((d, ff), F32),
+            pltpu.VMEM((ff, d), F32),
+            dma((8 * chunks + 1,)),
         ],
-        out_specs=(
-            pl.BlockSpec((rows, d), fixed),
-            pl.BlockSpec((d // steps, ff), lambda i: (i, 0)),
-            pl.BlockSpec((ff // steps, d), lambda i: (i, 0)),
-        ),
-    )(cot, full, pre_act, gp, gi)
+    )(*(pltpu.with_memory_space_constraint(x, pltpu.VMEM) for x in (cot, full, act, gp, gi)))
 
 
 def plain(inputs, cotangent, pre_act, w_up, w_down):

time: 35.1 us -> 32 us (0.912)
  Pallas kernels: 34 us -> 31.1 us
    pallas_call x1, Pallas kernels: 8.37 us -> 6.29 us  [fused(): pl.pallas_call(functools.partial(outer, chunks), out_shape=(jax.ShapeDtyp...]
    pallas_call x1, Pallas kernels: 25.6 us -> 24.8 us  [fused(): pl.pallas_call(functools.partial(exchange, n, chips, chunks), out_shape=(...]
where the time goes in v2:
time: 32 us; the launch traced here: 31.8 us
  Pallas kernels  31.1 us (97%)
  between operations  0.64 us (2%)
    pallas_call x1, Pallas kernels, fused(): pl.pallas_call(functools.partial(exchange, n, chips, chunks), out_shape=(...  24.8 us
    pallas_call x1, Pallas kernels, fused(): pl.pallas_call(functools.partial(outer, chunks), out_shape=(jax.ShapeDtyp...  6.29 us

profile of v2, /device:TPU:0, one launch (start us, length us, event | category | flops | bytes accessed | tf_op | source)
XLA Modules:
  0.0 31.8 jit_solution(2035148087698103491)
XLA Ops:
  0.6 24.8 %shard_map.76 = (bf16[48,1024]{1,0:T(8,128)(2,1)S(1)}, bf16[48,1024]{1,0:T(8,128)(2,1)S(1)}, bf16[4,48,512]{2,1,0:T(8,128)(2,1)S(1)}, bf16[4,48,512]{2,1,0:T(8,128)(2,1)S(1)}, bf16[6,1024]{1,0:T(8,128)(2,1)S(1)}) custom-call(bf16[6,1024]{1,0:T(8,128)(2,1)} %cot_ref.1, bf16[6,1024]{1,0:T(8,128)(2,1)} %in_ref.1, bf16[48,2048]{1,0:T(8,128)(2,1)} %pre_ref.1, ...), custom_call_target="tpu_custom_call" | custom-call | tf_op jit(solution)/shard_map/pallas_call | solution.py:297
  25.5 6.3 %shard_map.77 = (bf16[6,1024]{1,0:T(8,128)(2,1)}, f32[1024,2048]{1,0:T(8,128)}, f32[2048,1024]{1,0:T(8,128)}) custom-call(bf16[48,1024]{1,0:T(8,128)(2,1)S(1)} %get-tuple-element.8.cot_v, bf16[48,1024]{1,0:T(8,128)(2,1)S(1)} %get-tuple-element.9.in_v, bf16[4,48,512]{2,1,0:T(8,128)(2,1)S(1)} %get-tuple-element.10.act_v, ...), custom_call_target="tpu_custom_call" | custom-call | tf_op jit(solution)/shard_map/pallas_call | solution.py:340

commit v3 on v2

--- a/solution.py
+++ b/solution.py
@@ -126,13 +126,6 @@
         )
         copy.start()
         sends_c.append(copy)
-    for k in range(1, n):
-        copy = pltpu.make_async_remote_copy(
-            in_v, in_g.at[me], is_.at[k], ir.at[k], device_id={"fs": fs_peer[k]}
-        )
-        copy.start()
-        sends_i.append(copy)
-
     def picker(shape, token_dim):
         t = lax.broadcasted_iota(jnp.int32, shape, token_dim)
         j = lax.broadcasted_iota(jnp.int32, shape, 1 - token_dim)
@@ -182,6 +175,12 @@
             send2.append(copy)
 
     to_partner(0)
+    for k in range(1, n):
+        copy = pltpu.make_async_remote_copy(
+            in_v, in_g.at[me], is_.at[k], ir.at[k], device_id={"fs": fs_peer[k]}
+        )
+        copy.start()
+        sends_i.append(copy)
     for j in range(chunks):
         own[j] = dot(cot_out[...], wd_v[first + j], NT)
         if j + 1 < chunks:

time: 32 us -> 31.1 us (0.972)
  Pallas kernels: 31.1 us -> 30.2 us
    pallas_call x1, Pallas kernels: 24.8 us -> 23.9 us  [fused(): pl.pallas_call(functools.partial(exchange, n, chips, chunks), out_shape=(...]
where the time goes in v3:
time: 31.1 us; the launch traced here: 30.8 us
  Pallas kernels  30.2 us (97%)
  between operations  0.64 us (2%)
    pallas_call x1, Pallas kernels, fused(): pl.pallas_call(functools.partial(exchange, n, chips, chunks), out_shape=(...  23.9 us
    pallas_call x1, Pallas kernels, fused(): pl.pallas_call(functools.partial(outer, chunks), out_shape=(jax.ShapeDtyp...  6.29 us

profile of v3, /device:TPU:0, one launch (start us, length us, event | category | flops | bytes accessed | tf_op | source)
XLA Modules:
  0.0 30.8 jit_solution(6082693231599375201)
XLA Ops:
  0.6 23.9 %shard_map.76 = (bf16[48,1024]{1,0:T(8,128)(2,1)S(1)}, bf16[48,1024]{1,0:T(8,128)(2,1)S(1)}, bf16[4,48,512]{2,1,0:T(8,128)(2,1)S(1)}, bf16[4,48,512]{2,1,0:T(8,128)(2,1)S(1)}, bf16[6,1024]{1,0:T(8,128)(2,1)S(1)}) custom-call(bf16[6,1024]{1,0:T(8,128)(2,1)} %cot_ref.1, bf16[6,1024]{1,0:T(8,128)(2,1)} %in_ref.1, bf16[48,2048]{1,0:T(8,128)(2,1)} %pre_ref.1, ...), custom_call_target="tpu_custom_call" | custom-call | tf_op jit(solution)/shard_map/pallas_call | solution.py:296
  24.5 6.3 %shard_map.77 = (bf16[6,1024]{1,0:T(8,128)(2,1)}, f32[1024,2048]{1,0:T(8,128)}, f32[2048,1024]{1,0:T(8,128)}) custom-call(bf16[48,1024]{1,0:T(8,128)(2,1)S(1)} %get-tuple-element.8.cot_v, bf16[48,1024]{1,0:T(8,128)(2,1)S(1)} %get-tuple-element.9.in_v, bf16[4,48,512]{2,1,0:T(8,128)(2,1)S(1)} %get-tuple-element.10.act_v, ...), custom_call_target="tpu_custom_call" | custom-call | tf_op jit(solution)/shard_map/pallas_call | solution.py:339
